TPU v7x, 32 devices: a whole 2x2x4 slice. The times are simulated.
32 devices in a mesh: sp: 8 (over z, y), tp: 4 (over x, core).
Axes of the slice: x: 2, y: 2, z: 4, core: 2. Of those that a mesh axis runs over, the one named last changes fastest.
Arguments:
- inputs: bfloat16 [4096, 4096], P('sp', 'tp'), may hold values from -24 to 24
- length: int32 [1], replicated, may hold values from 2049 to 4096
- win_query: bfloat16 [4096, 1536], P(None, 'tp'), may hold values from -8 to 8
- win_key: bfloat16 [4096, 512], P(None, 'tp'), may hold values from -8 to 8
- win_value: bfloat16 [4096, 512], P(None, 'tp'), may hold values from -1.5 to 1.5
- sink_logit: float32 [24], P('tp'), may hold values from 4 to 8
- diff_query: bfloat16 [4096, 1024], P(None, 'tp'), may hold values from -8 to 8
- diff_key: bfloat16 [4096, 1024], P(None, 'tp'), may hold values from -8 to 8
- diff_value: bfloat16 [4096, 1024], P(None, 'tp'), may hold values from -0.09375 to 0.09375
- mix_lambda: float32 [16], P('tp'), may hold values from 0.3 to 0.8
- head_gain: float32 [64], replicated, may hold values from 0.1 to 1.9
- win_out: bfloat16 [1536, 4096], P('tp'), may hold values from -0.125 to 0.125
- diff_out: bfloat16 [1024, 4096], P('tp'), may hold values from -0.125 to 0.125
Outputs:
- merged_out: bfloat16 [4096, 4096], P(('sp', 'tp'))
All inputs are finite; a program needn't handle non-finite values.
Results may differ from a plain program's by a relative error of at most 0.015.
Values may be sent and summed in bfloat16 or wider, within the bound.
No kernel may reach another device: no remote copies, remote signals or barrier semaphores. Data moves between devices by JAX's collectives and lax.ppermute only.
A program may use at most 128 MiB of HBM per device.

v0:
```python
import jax
import jax.numpy as jnp
from jax import lax
from jax.sharding import PartitionSpec as P

HEAD = 64
DQK = 32
GROUP = 3
WINDOW = 128
epsilon = 1e-06
masked_score = -1e30


def extended(block, sides, width):
    for axis, dim in sides:
        count = lax.axis_size(axis)
        forward = [(i, i + 1) for i in range(count - 1)]
        backward = [(target, source) for source, target in forward]
        low = lax.ppermute(
            lax.slice_in_dim(block, block.shape[dim] - width, None, axis=dim), axis, forward
        )
        high = lax.ppermute(lax.slice_in_dim(block, 0, width, axis=dim), axis, backward)
        block = jnp.concatenate([low, block, high], axis=dim)
    return block


def window_part(win_q, win_k, win_v, sink_logit, live_count, offset):
    row_count = win_q.shape[0]
    kv_local = win_k.shape[1] // HEAD
    stacked = jnp.stack(
        (win_k.reshape(row_count, kv_local, HEAD), win_v.reshape(row_count, kv_local, HEAD)), axis=2
    )
    stacked = stacked.reshape(row_count, kv_local * 2 * HEAD)
    padded = extended(stacked, (("sp", 0),), WINDOW)
    padded = padded.reshape(row_count + 2 * WINDOW, kv_local, 2, HEAD)
    keys_win = padded[:, :, 0]
    values_win = padded[:, :, 1]
    queries = win_q.reshape(row_count, kv_local, GROUP, HEAD)
    sink_table = sink_logit.reshape(kv_local, GROUP)
    query_pos = offset + jnp.arange(row_count, dtype=jnp.int32)
    key_pos = offset - WINDOW + jnp.arange(row_count + 2 * WINDOW, dtype=jnp.int32)
    allowed = (
        (jnp.abs(query_pos[:, None] - key_pos[None, :]) <= WINDOW)
        & (key_pos[None, :] >= 0)
        & (key_pos[None, :] < live_count)
    )
    scores = jnp.einsum(
        "qhgd,khd->hgqk", queries, keys_win, preferred_element_type=jnp.float32
    ) * HEAD ** (-0.5)
    scores = jnp.where(allowed[None, None], scores, masked_score)
    row_max = jnp.maximum(jnp.max(scores, axis=-1), sink_table[:, :, None])
    exponent = jnp.where(allowed[None, None], jnp.exp(scores - row_max[..., None]), 0.0)
    denominator = jnp.sum(exponent, axis=-1) + jnp.exp(sink_table[:, :, None] - row_max)
    result = jnp.einsum(
        "hgqk,khd->qhgd",
        exponent.astype(jnp.bfloat16),
        values_win,
        preferred_element_type=jnp.float32,
    )
    result = result / jnp.transpose(denominator, (2, 0, 1))[..., None]
    result = jnp.where((query_pos < live_count)[:, None, None, None], result, 0.0)
    return result.reshape(row_count, kv_local * GROUP * HEAD).astype(jnp.bfloat16)


def attend(running, queries, key_part, value_part, live_count, block_total, query_step):
    key_length = key_part.shape[0]
    key_step = 4096

    def one_query_block(block_index, block_state):
        running_max, total_sum, weighted = block_state
        row_begin = block_index * query_step
        query_slab = lax.dynamic_slice_in_dim(queries, row_begin, query_step, 0)
        start_state = (
            lax.dynamic_slice_in_dim(running_max, row_begin, query_step, 2),
            lax.dynamic_slice_in_dim(total_sum, row_begin, query_step, 2),
            lax.dynamic_slice_in_dim(weighted, row_begin, query_step, 2),
        )

        def one_key_block(key_index, key_state):
            block_max, block_sum, block_weighted = key_state
            key_begin = key_index * key_step
            key_slab = lax.dynamic_slice_in_dim(key_part, key_begin, key_step, 0)
            value_slab = lax.dynamic_slice_in_dim(value_part, key_begin, key_step, 0)
            key_pos = key_begin + jnp.arange(key_step, dtype=jnp.int32)
            allowed = key_pos < live_count
            scores = jnp.einsum(
                "qhmd,khmd->hmqk", query_slab, key_slab, preferred_element_type=jnp.float32
            ) * DQK ** (-0.5)
            scores = jnp.where(allowed, scores, masked_score)
            new_max = jnp.maximum(block_max, jnp.max(scores, axis=-1))
            rescale = jnp.exp(block_max - new_max)
            exponent = jnp.where(allowed, jnp.exp(scores - new_max[..., None]), 0.0)
            new_total = block_sum * rescale + jnp.sum(exponent, axis=-1)
            new_weighted = block_weighted * rescale[..., None] + jnp.einsum(
                "hmqk,khd->hmqd",
                exponent.astype(jnp.bfloat16),
                value_slab,
                preferred_element_type=jnp.float32,
            )
            return (new_max, new_total, new_weighted)

        final_state = lax.fori_loop(0, key_length // key_step, one_key_block, start_state)
        return (
            lax.dynamic_update_slice_in_dim(running_max, final_state[0], row_begin, 2),
            lax.dynamic_update_slice_in_dim(total_sum, final_state[1], row_begin, 2),
            lax.dynamic_update_slice_in_dim(weighted, final_state[2], row_begin, 2),
        )

    return lax.fori_loop(0, block_total, one_query_block, running)


def diff_part(diff_q, diff_k, diff_v, mix_lambda, head_gain, live_count, offset):
    row_count = diff_q.shape[0]
    heads_local = mix_lambda.shape[0]
    query_step = 128
    positions = offset + jnp.arange(row_count, dtype=jnp.int32)
    live_rows = jnp.sum((positions < live_count).astype(jnp.int32))
    block_total = (live_rows + query_step - 1) // query_step
    queries = diff_q.reshape(row_count, heads_local, 2, DQK)
    zero_state = (
        jnp.full((heads_local, 2, row_count), masked_score, jnp.float32),
        jnp.zeros((heads_local, 2, row_count), jnp.float32),
        jnp.zeros((heads_local, 2, row_count, HEAD), jnp.float32),
    )
    key_part = lax.all_gather(diff_k, "sp", axis=0, tiled=True).reshape(-1, heads_local, 2, DQK)
    value_part = lax.all_gather(diff_v, "sp", axis=0, tiled=True).reshape(-1, heads_local, HEAD)
    running = lax.cond(
        jnp.int32(0) < live_count,
        lambda inner_state: attend(
            inner_state, queries, key_part, value_part, live_count, block_total, query_step
        ),
        lambda inner_state: inner_state,
        zero_state,
    )
    total_sum = running[1]
    safe_total = jnp.where(total_sum > 0.0, total_sum, 1.0)
    map_rows = running[2] / safe_total[..., None]
    mixed_rows = map_rows[:, 0] - mix_lambda[:, None, None] * map_rows[:, 1]
    normed = (
        mixed_rows
        * lax.rsqrt(jnp.mean(mixed_rows * mixed_rows, axis=-1, keepdims=True) + epsilon)
        * head_gain
    )
    normed = jnp.where((positions < live_count)[None, :, None], normed, 0.0)
    result = (
        jnp.transpose(normed, (1, 0, 2)).reshape(row_count, heads_local * HEAD).astype(jnp.bfloat16)
    )
    return result


def body(
    inputs,
    length,
    win_query,
    win_key,
    win_value,
    sink_logit,
    diff_query,
    diff_key,
    diff_value,
    mix_lambda,
    head_gain,
    win_out,
    diff_out,
):
    row_count = inputs.shape[0]
    live_count = length[0]
    weights = (win_query, win_key, win_value, diff_query, diff_key, diff_value)
    segment = lax.all_gather(inputs, "tp", axis=1, tiled=True)
    summed = tuple(
        (jnp.dot(segment, weight, preferred_element_type=jnp.float32) for weight in weights)
    )
    win_q, win_k, win_v, diff_q, diff_k, diff_v = [total.astype(jnp.bfloat16) for total in summed]
    offset = lax.axis_index("sp") * row_count
    win_rows = window_part(win_q, win_k, win_v, sink_logit, live_count, offset)
    diff_rows = diff_part(diff_q, diff_k, diff_v, mix_lambda, head_gain, live_count, offset)
    partial_value = jnp.dot(win_rows, win_out, preferred_element_type=jnp.float32)
    return lax.psum_scatter(
        (partial_value + jnp.dot(diff_rows, diff_out, preferred_element_type=jnp.float32)).astype(
            jnp.bfloat16
        ),
        "tp",
        scatter_dimension=0,
        tiled=True,
    )


def solution(mesh):
    placed = (
        P("sp", "tp"),
        P(),
        P(None, "tp"),
        P(None, "tp"),
        P(None, "tp"),
        P("tp"),
        P(None, "tp"),
        P(None, "tp"),
        P(None, "tp"),
        P("tp"),
        P(),
        P("tp", None),
        P("tp", None),
    )
    return jax.shard_map(
        body, mesh=mesh, in_specs=placed, out_specs=P(("sp", "tp"), None), check_vma=False
    )
```

profile of v0, /device:TPU:0, one launch (start us, length us, event | category | flops | bytes accessed | tf_op | source)
XLA Modules:
  0.0 299.4 jit_solution(1611999572940378291)
XLA Ops:
  7.3 38.8 %all-gather.4.cloned.1.call-done = bf16[512,4096]{1,0:T(8,128)(2,1)} async-done(((bf16[512,1024]{1,0:T(8,128)(2,1)}), bf16[512,4096]{1,0:T(8,128)(2,1)}) %all-gather.4.cloned.1.call-update) | async-done | bytes 4194320 | tf_op jit(solution)/shard_map/all_gather | solution.py:169
  46.1 4.8 %convolution_convert_fusion.1 = bf16[512,256]{1,0:T(8,128)(2,1)} fusion(bf16[512,4096]{1,0:T(8,128)(2,1)} %all-gather.4.cloned.1.call-done, bf16[4096,256]{1,0:T(8,128)(2,1)} %param.25), kind=kOutput, calls=%fused_computation.34 | convolution fusion | flops 1073872896 | bytes 6553600 | tf_op jit(solution)/shard_map/dot_general | solution.py:171
  52.6 4.4 %convolution_convert_fusion.4 = bf16[512,128]{0,1:T(8,128)(2,1)S(1)} fusion(bf16[512,4096]{1,0:T(8,128)(2,1)} %all-gather.4.cloned.1.call-done, bf16[4096,128]{1,0:T(8,128)(2,1)} %param.21), kind=kOutput, calls=%fused_computation.37 | convolution fusion | flops 536936448 | bytes 5373952 | tf_op jit(solution)/shard_map/dot_general | solution.py:171
  57.0 1.5 convolution_convert_fusion.5
  61.8 5.2 %collective-permute-start = (bf16[128,256]{0,1:T(8,128)(2,1)}, bf16[128,256]{0,1:T(8,128)(2,1)}, u32[]{:S(2)}, u32[]{:S(2)}) collective-permute-start(bf16[128,256]{0,1:T(8,128)(2,1)} %bitcast.8), channel_id=1, source_target_pairs={{0,4},{4,8},{8,12},{12,16},{16,20},{20,24},{24,28},{1,5},{5,9},{9,... | collective-permute-start | bytes 196616 | tf_op jit(solution)/shard_map/ppermute | solution.py:19
  67.0 2.0 convolution_convert_fusion.2
  69.2 5.2 %convolution_convert_fusion = bf16[512,384]{0,1:T(8,128)(2,1)S(1)} fusion(bf16[512,4096]{1,0:T(8,128)(2,1)} %all-gather.4.cloned.1.call-done, bf16[4096,384]{1,0:T(8,128)(2,1)} %param.19), kind=kOutput, calls=%fused_computation.33 | convolution fusion | flops 1610809344 | bytes 7733248 | tf_op jit(solution)/shard_map/dot_general | solution.py:171
  74.4 2.0 convolution_convert_fusion.3
  77.3 1.7 fusion.23
  79.1 2.3 fusion.24
  81.4 2.7 fusion.40
  84.1 5.6 %fusion.52 = f32[512,4096]{1,0:T(8,128)} fusion(bf16[512,384]{0,1:T(8,128)(2,1)S(1)} %bitcast.123, bf16[384,4096]{1,0:T(8,128)(2,1)S(1)} %copy-done), kind=kOutput, calls=%fused_computation.68 | convolution fusion | flops 1610612736 | bytes 11927552 | tf_op jit(solution)/shard_map/dot_general | solution.py:177
  89.7 11.3 %all-gather.8.cloned.1.call-done = bf16[4096,256]{1,0:T(8,128)(2,1)} async-done(((bf16[512,256]{1,0:T(8,128)(2,1)}), bf16[4096,256]{1,0:T(8,128)(2,1)}) %all-gather.8.cloned.1.call-update) | async-done | bytes 2097168 | tf_op jit(solution)/shard_map/all_gather | solution.py:126
  101.0 49.8 %all-gather.6.cloned.1.call-done = bf16[4096,256]{1,0:T(8,128)(2,1)} async-done(((bf16[512,256]{1,0:T(8,128)(2,1)}), bf16[4096,256]{1,0:T(8,128)(2,1)}) %all-gather.6.cloned.1.call-update) | async-done | bytes 2097168 | tf_op jit(solution)/shard_map/all_gather | solution.py:125
  150.8 89.2 %conditional.1 = (f32[4,2,512]{2,1,0:T(2,128)}, f32[4,2,512,64]{2,3,1,0:T(8,128)}) conditional(s32[]{:T(128)} %convert_element_type.55, () %tuple.34, (s32[512]{0:T(512)S(1)}, bf16[512,256]{1,0:T(8,128)(2,1)S(1)}, bf16[4096,256]{1,0:T(8,128)(2,1)}, bf16[4096,256]{1,0:T(8,128)(2,1)}, s32[]{:T(128)}, /*index=5*/s32[]{:T(128)}) %tuple.79), branch_computations={%region_3.4_spmd, %region_4.9_spmd.clone} | conditional | flops 859970048 | bytes 132364824 | solution.py:127
  152.3 4.1 %copy.34 = bf16[4096,256]{0,1:T(8,128)(2,1)} copy(bf16[4096,256]{1,0:T(8,128)(2,1)} %get-tuple-element.250) | data formatting | bytes 4194304 | tf_op jit(solution)/shard_map
  156.4 2.9 copy.33
  161.0 79.0 %while.37 = (s32[]{:T(128)}, f32[4,2,512]{2,1,0:T(2,128)S(1)}, f32[4,2,512]{2,1,0:T(2,128)}, f32[4,2,512,64]{2,3,1,0:T(8,128)}, s32[]{:T(128)}, /*index=5*/s32[]...) while((s32[]{:T(128)}, f32[4,2,512]{2,1,0:T(2,128)S(1)}, ...), condition=%wide.region_8.8_spmd, body=%wide.region_5.7_spmd.sunk | while | flops 859969536 | bytes 122368224 | solution.py:109
  161.7 2.7 fusion.82
  164.5 4.9 %fusion.83 = f32[4,2,128]{2,1,0:T(2,128)S(1)} fusion(f32[4,2,128,4096]{3,2,1,0:T(8,128)S(1)} %get-tuple-element.357, f32[4,2,128]{2,1,0:T(2,128)S(1)} %get-tuple-element.358, pred[4096]{0:T(1024)(128)(4,1)S(1)} %iota_compare_fusion.2), kind=kLoop, calls=%fused_computation.4.clone.1 | loop fusion | flops 20970496 | bytes 16789504 | tf_op jit(solution)/shard_map/cond/branch_1_fun/while/body/while/body/eval_jaxpr/reduce_sum | solution.py:93
  171.5 9.3 %fusion.84 = f32[4,2,512,64]{2,3,1,0:T(8,128)} fusion(f32[4,2,512,64]{2,3,1,0:T(8,128)} %get-tuple-element.377, s32[]{:T(128)S(6)} %select_n.128, bf16[4096,4,64]{0,2,1:T(8,128)(2,1)} %get-tuple-element.395, f32[4,2,128,4096]{3,2,1,0:T(8,128)} %copy-done.2, f32[4,2,128]{2,1,0:T(2,128)S(1)} %get-tuple-element.358, ...), kind=kOutput, calls=%fused_computation.9.clone.1 | convolution fusion | flops 557973504 | bytes 19410948 | tf_op jit(solution)/shard_map/cond/branch_1_fun/while/body/while/body/eval_jaxpr/hmqk,khd->hmqd/dot_general | solution.py:94
  181.5 2.7 fusion.82
  184.2 4.9 %fusion.83 = f32[4,2,128]{2,1,0:T(2,128)S(1)} fusion(f32[4,2,128,4096]{3,2,1,0:T(8,128)S(1)} %get-tuple-element.357, f32[4,2,128]{2,1,0:T(2,128)S(1)} %get-tuple-element.358, pred[4096]{0:T(1024)(128)(4,1)S(1)} %iota_compare_fusion.2), kind=kLoop, calls=%fused_computation.4.clone.1 | loop fusion | flops 20970496 | bytes 16789504 | tf_op jit(solution)/shard_map/cond/branch_1_fun/while/body/while/body/eval_jaxpr/reduce_sum | solution.py:93
  191.2 9.3 %fusion.84 = f32[4,2,512,64]{2,3,1,0:T(8,128)} fusion(f32[4,2,512,64]{2,3,1,0:T(8,128)} %get-tuple-element.377, s32[]{:T(128)S(6)} %select_n.128, bf16[4096,4,64]{0,2,1:T(8,128)(2,1)} %get-tuple-element.395, f32[4,2,128,4096]{3,2,1,0:T(8,128)} %copy-done.2, f32[4,2,128]{2,1,0:T(2,128)S(1)} %get-tuple-element.358, ...), kind=kOutput, calls=%fused_computation.9.clone.1 | convolution fusion | flops 557973504 | bytes 19410948 | tf_op jit(solution)/shard_map/cond/branch_1_fun/while/body/while/body/eval_jaxpr/hmqk,khd->hmqd/dot_general | solution.py:94
  201.2 2.7 fusion.82
  204.0 4.9 %fusion.83 = f32[4,2,128]{2,1,0:T(2,128)S(1)} fusion(f32[4,2,128,4096]{3,2,1,0:T(8,128)S(1)} %get-tuple-element.357, f32[4,2,128]{2,1,0:T(2,128)S(1)} %get-tuple-element.358, pred[4096]{0:T(1024)(128)(4,1)S(1)} %iota_compare_fusion.2), kind=kLoop, calls=%fused_computation.4.clone.1 | loop fusion | flops 20970496 | bytes 16789504 | tf_op jit(solution)/shard_map/cond/branch_1_fun/while/body/while/body/eval_jaxpr/reduce_sum | solution.py:93
  211.0 9.3 %fusion.84 = f32[4,2,512,64]{2,3,1,0:T(8,128)} fusion(f32[4,2,512,64]{2,3,1,0:T(8,128)} %get-tuple-element.377, s32[]{:T(128)S(6)} %select_n.128, bf16[4096,4,64]{0,2,1:T(8,128)(2,1)} %get-tuple-element.395, f32[4,2,128,4096]{3,2,1,0:T(8,128)} %copy-done.2, f32[4,2,128]{2,1,0:T(2,128)S(1)} %get-tuple-element.358, ...), kind=kOutput, calls=%fused_computation.9.clone.1 | convolution fusion | flops 557973504 | bytes 19410948 | tf_op jit(solution)/shard_map/cond/branch_1_fun/while/body/while/body/eval_jaxpr/hmqk,khd->hmqd/dot_general | solution.py:94
  221.0 2.7 fusion.82
  223.7 4.9 %fusion.83 = f32[4,2,128]{2,1,0:T(2,128)S(1)} fusion(f32[4,2,128,4096]{3,2,1,0:T(8,128)S(1)} %get-tuple-element.357, f32[4,2,128]{2,1,0:T(2,128)S(1)} %get-tuple-element.358, pred[4096]{0:T(1024)(128)(4,1)S(1)} %iota_compare_fusion.2), kind=kLoop, calls=%fused_computation.4.clone.1 | loop fusion | flops 20970496 | bytes 16789504 | tf_op jit(solution)/shard_map/cond/branch_1_fun/while/body/while/body/eval_jaxpr/reduce_sum | solution.py:93
  230.7 9.3 %fusion.84 = f32[4,2,512,64]{2,3,1,0:T(8,128)} fusion(f32[4,2,512,64]{2,3,1,0:T(8,128)} %get-tuple-element.377, s32[]{:T(128)S(6)} %select_n.128, bf16[4096,4,64]{0,2,1:T(8,128)(2,1)} %get-tuple-element.395, f32[4,2,128,4096]{3,2,1,0:T(8,128)} %copy-done.2, f32[4,2,128]{2,1,0:T(2,128)S(1)} %get-tuple-element.358, ...), kind=kOutput, calls=%fused_computation.9.clone.1 | convolution fusion | flops 557973504 | bytes 19410948 | tf_op jit(solution)/shard_map/cond/branch_1_fun/while/body/while/body/eval_jaxpr/hmqk,khd->hmqd/dot_general | solution.py:94
  242.7 6.8 %add_convert_fusion = bf16[512,4096]{1,0:T(8,128)(2,1)} fusion(f32[512,4096]{1,0:T(8,128)} %fusion.52, bf16[512,256]{0,1:T(8,128)(2,1)S(1)} %bitcast.122, bf16[256,4096]{1,0:T(8,128)(2,1)S(1)} %copy-done.5), kind=kOutput, calls=%fused_computation.23 | convolution fusion | flops 1077936128 | bytes 14942208 | tf_op jit(solution)/shard_map/dot_general | solution.py:179
  249.6 43.2 %reduce-scatter.2.cloned.1.call-done = bf16[128,4096]{1,0:T(8,128)(2,1)} async-done(((bf16[512,4096]{1,0:T(8,128)(2,1)}), bf16[128,4096]{1,0:T(8,128)(2,1)}) %reduce-scatter.2.cloned.1.call-update) | async-done | bytes 1048592 | tf_op jit(solution)/shard_map/reduce_scatter | solution.py:178
  (93 shorter events, 22.6 us)
Async XLA Ops:
  6.5 77.6 %copy-start = (bf16[384,4096]{1,0:T(8,128)(2,1)S(1)}, bf16[384,4096]{1,0:T(8,128)(2,1)}, u32[]{:S(2)}) copy-start(bf16[384,4096]{1,0:T(8,128)(2,1)} %param.28) | copy-start | bytes 9437188
  6.5 39.6 %all-gather.4.cloned.1.call-start = ((), (), s32[]{:S(2)}) async-start(), calls=%async_computation.1 | async-start | bytes 5242880 | tf_op jit(solution)/shard_map/all_gather | solution.py:169
  7.3 44.4 %copy-start.16 = (f32[6]{0:T(128)S(1)}, f32[6]{0:T(128)}, u32[]{:S(2)}) copy-start(f32[6]{0:T(128)} %param.22) | copy-start | bytes 76
  7.3 93.7 %all-gather.8.cloned.1.call-start = ((), (), s32[]{:S(2)}) async-start(), calls=%async_computation.3 | async-start | bytes 2359296 | tf_op jit(solution)/shard_map/all_gather | solution.py:126
  51.0 99.8 %all-gather.6.cloned.1.call-start = ((), (), s32[]{:S(2)}) async-start(), calls=%async_computation.2 | async-start | bytes 2359296 | tf_op jit(solution)/shard_map/all_gather | solution.py:125
  51.8 5.2 %copy-start.3 = (bf16[512,4096]{1,0:T(8,128)(2,1)S(1)}, bf16[512,4096]{1,0:T(8,128)(2,1)}, u32[]{:S(2)}) copy-start(bf16[512,4096]{1,0:T(8,128)(2,1)} %all-gather.4.cloned.1.call-done) | copy-start | bytes 12582916
  51.8 5.2 %copy-start.10 = (bf16[4096,128]{1,0:T(8,128)(2,1)S(1)}, bf16[4096,128]{1,0:T(8,128)(2,1)}, u32[]{:S(2)}) copy-start(bf16[4096,128]{1,0:T(8,128)(2,1)} %param.20) | copy-start | bytes 3145732
  57.0 1.5 copy-start.6
  57.0 9.9 %copy-start.14 = (bf16[4096,256]{1,0:T(8,128)(2,1)S(1)}, bf16[4096,256]{1,0:T(8,128)(2,1)}, u32[]{:S(2)}) copy-start(bf16[4096,256]{1,0:T(8,128)(2,1)} %param.24) | copy-start | bytes 6291460
  58.6 0.7 copy-start.8
  60.5 15.9 %collective-permute-start.1 = (bf16[128,256]{0,1:T(8,128)(2,1)}, bf16[128,256]{0,1:T(8,128)(2,1)}, u32[]{:S(2)}, u32[]{:S(2)}) collective-permute-start(bf16[128,256]{0,1:T(8,128)(2,1)} %bitcast.10), channel_id=1, source_target_pairs={{4,0},{8,4},{12,8},{16,12},{20,16},{24,20},{28,24},{5,1},{9,5},{13... | collective-permute-start | bytes 196616 | tf_op jit(solution)/shard_map/ppermute | solution.py:22
  61.8 14.6 %collective-permute-start = (bf16[128,256]{0,1:T(8,128)(2,1)}, bf16[128,256]{0,1:T(8,128)(2,1)}, u32[]{:S(2)}, u32[]{:S(2)}) collective-permute-start(bf16[128,256]{0,1:T(8,128)(2,1)} %bitcast.8), channel_id=1, source_target_pairs={{0,4},{4,8},{8,12},{12,16},{16,20},{20,24},{24,28},{1,5},{5,9},{9,... | collective-permute-start | bytes 196616 | tf_op jit(solution)/shard_map/ppermute | solution.py:19
  69.0 223.9 %reduce-scatter.2.cloned.1.call-start = ((), (), s32[]{:S(2)}) async-start(), calls=%async_computation.4 | async-start | bytes 5242880 | tf_op jit(solution)/shard_map/reduce_scatter | solution.py:178
  69.2 5.2 %copy-start.4 = (bf16[512,4096]{1,0:T(8,128)(2,1)S(1)}, bf16[512,4096]{1,0:T(8,128)(2,1)}, u32[]{:S(2)}) copy-start(bf16[512,4096]{1,0:T(8,128)(2,1)} %all-gather.4.cloned.1.call-done) | copy-start | bytes 12582916
  69.2 5.2 %copy-start.15 = (bf16[4096,256]{1,0:T(8,128)(2,1)S(1)}, bf16[4096,256]{1,0:T(8,128)(2,1)}, u32[]{:S(2)}) copy-start(bf16[4096,256]{1,0:T(8,128)(2,1)} %param.23) | copy-start | bytes 6291460
  74.4 2.0 copy-start.7
  74.4 2.0 copy-start.9
  84.1 66.7 %copy-start.11 = (bf16[512,256]{1,0:T(8,128)(2,1)S(1)}, bf16[512,256]{1,0:T(8,128)(2,1)}, u32[]{:S(2)}) copy-start(bf16[512,256]{1,0:T(8,128)(2,1)} %convolution_convert_fusion.3) | copy-start | bytes 786436
  150.8 91.5 %copy-start.12 = (f32[4]{0:T(128)S(1)}, f32[4]{0:T(128)}, u32[]{:S(2)}) copy-start(f32[4]{0:T(128)} %param.26) | copy-start | bytes 52
  150.8 91.7 %copy-start.13 = (f32[64]{0:T(128)S(1)}, f32[64]{0:T(128)}, u32[]{:S(2)}) copy-start(f32[64]{0:T(128)} %param.27) | copy-start | bytes 772
  164.4 5.7 %copy-start.2 = (f32[4,2,128,4096]{3,2,1,0:T(8,128)}, f32[4,2,128,4096]{3,2,1,0:T(8,128)S(1)}, u32[]{:S(2)}) copy-start(f32[4,2,128,4096]{3,2,1,0:T(8,128)S(1)} %get-tuple-element.357) | copy-start | bytes 50331652 | tf_op jit(solution)/shard_map/cond/branch_1_fun/while
  184.2 5.7 %copy-start.2 = (f32[4,2,128,4096]{3,2,1,0:T(8,128)}, f32[4,2,128,4096]{3,2,1,0:T(8,128)S(1)}, u32[]{:S(2)}) copy-start(f32[4,2,128,4096]{3,2,1,0:T(8,128)S(1)} %get-tuple-element.357) | copy-start | bytes 50331652 | tf_op jit(solution)/shard_map/cond/branch_1_fun/while
  204.0 5.7 %copy-start.2 = (f32[4,2,128,4096]{3,2,1,0:T(8,128)}, f32[4,2,128,4096]{3,2,1,0:T(8,128)S(1)}, u32[]{:S(2)}) copy-start(f32[4,2,128,4096]{3,2,1,0:T(8,128)S(1)} %get-tuple-element.357) | copy-start | bytes 50331652 | tf_op jit(solution)/shard_map/cond/branch_1_fun/while
  223.7 5.7 %copy-start.2 = (f32[4,2,128,4096]{3,2,1,0:T(8,128)}, f32[4,2,128,4096]{3,2,1,0:T(8,128)S(1)}, u32[]{:S(2)}) copy-start(f32[4,2,128,4096]{3,2,1,0:T(8,128)S(1)} %get-tuple-element.357) | copy-start | bytes 50331652 | tf_op jit(solution)/shard_map/cond/branch_1_fun/while
  240.1 2.7 copy-start.5
  242.7 50.1 %copy-start.1 = (bf16[384,4096]{1,0:T(8,128)(2,1)S(1)}, bf16[384,4096]{1,0:T(8,128)(2,1)}, u32[]{:S(2)}) copy-start(bf16[384,4096]{1,0:T(8,128)(2,1)} %param.28) | copy-start | bytes 9437188
Sparse Core Ops, SparseCore 0:
  8.9 37.1 all-gather.3
  51.1 49.8 all-gather.7
  103.1 47.6 all-gather.5
  249.7 43.0 reduce-scatter.1
where the time goes:
time: 300 us; the launch traced here: 299 us
  waiting for transfers between devices  144 us (48%)
  matrix products  84.8 us (28%)
  other arithmetic  34.7 us (12%)
  local copies, waits for them, and re-layouts  14.3 us (5%)
  between operations  14.1 us (5%)
  starting transfers between devices  6.77 us (2%)
    all_gather x1, waiting for transfers between devices, diff_part(): lax.all_gather(diff_k, 'sp', axis=0, tiled=True)  49.8 us
    reduce_scatter x1, waiting for transfers between devices, body(): lax.psum_scatter((partial_value + jnp.dot(diff_rows, diff_out, preferred_...  43.2 us
    all_gather x1, waiting for transfers between devices, body(): segment = lax.all_gather(inputs, 'tp', axis=1, tiled=True)  38.8 us
    dot_general x4, matrix products, one_key_block(): jnp.einsum('hmqk,khd->hmqd', exponent.astype(jnp.bfloat16), value_slab, p...  37.3 us
    dot_general x6, matrix products, body(): jnp.dot(segment, weight, preferred_element_type=jnp.float32)  19.8 us
    reduce_sum x4, other arithmetic, one_key_block(): new_total = block_sum * rescale + jnp.sum(exponent, axis=-1)  19.5 us
    all_gather x1, waiting for transfers between devices, diff_part(): lax.all_gather(diff_v, 'sp', axis=0, tiled=True)  11.3 us
    dot_general x4, matrix products, one_key_block(): jnp.einsum('qhmd,khmd->hmqk', query_slab, key_slab, preferred_element_typ...  11 us
  transfers between devices with their start and end apart: 6, of which 4 were waited for; matrix products, arithmetic and copies ran while one was open for 10% of the time, Pallas kernels for 0%

commit v1 on v0

--- a/solution.py
+++ b/solution.py
@@ -166,7 +166,12 @@
     row_count = inputs.shape[0]
     live_count = length[0]
     weights = (win_query, win_key, win_value, diff_query, diff_key, diff_value)
-    segment = lax.all_gather(inputs, "tp", axis=1, tiled=True)
+    ring = [inputs]
+    for hop in range(3):
+        ring.append(lax.ppermute(ring[-1], "tp", [(dev, (dev + 1) % 4) for dev in range(4)]))
+    segment = jnp.roll(
+        jnp.concatenate(ring[::-1], axis=1), (lax.axis_index("tp") + 1) * ring[0].shape[1], axis=1
+    )
     summed = tuple(
         (jnp.dot(segment, weight, preferred_element_type=jnp.float32) for weight in weights)
     )

time: 300 us -> 316 us (1.053)
  local copies, waits for them, and re-layouts: 14.3 us -> 26.4 us
  matrix products: 84.8 us -> 88.6 us
    ppermute x0 -> x3, waiting for transfers between devices: none -> 43.4 us  [body(): lax.ppermute(ring[-1], 'tp', [(dev, (dev + 1) % 4) for dev in range(4)])]
    all_gather x1, waiting for transfers between devices: 49.8 us -> 6.7 us  [diff_part(): lax.all_gather(diff_k, 'sp', axis=0, tiled=True)]
    all_gather x1 -> x0, waiting for transfers between devices: 38.8 us -> none  [body(): segment = lax.all_gather(inputs, 'tp', axis=1, tiled=True)]
    all_gather x1, waiting for transfers between devices: 11.3 us -> 49.8 us  [diff_part(): lax.all_gather(diff_v, 'sp', axis=0, tiled=True)]
    unnamed x32 -> x39, local copies, waits for them, and re-layouts: 0.7 us -> 12.7 us
  transfers between devices with their start and end apart: 6 -> 8, of which waited for: 4 -> 6; matrix products, arithmetic and copies ran while one was open for 10% -> 12% of each run, Pallas kernels for 0% -> 0%
where the time goes in v1:
time: 316 us; the launch traced here: 315 us
  waiting for transfers between devices  143 us (45%)
  matrix products  88.6 us (28%)
  other arithmetic  34.7 us (11%)
  local copies, waits for them, and re-layouts  26.4 us (8%)
  between operations  14 us (4%)
  starting transfers between devices  7.58 us (2%)
    all_gather x1, waiting for transfers between devices, diff_part(): lax.all_gather(diff_v, 'sp', axis=0, tiled=True)  49.8 us
    ppermute x3, waiting for transfers between devices, body(): lax.ppermute(ring[-1], 'tp', [(dev, (dev + 1) % 4) for dev in range(4)])  43.4 us
    reduce_scatter x1, waiting for transfers between devices, body(): lax.psum_scatter((partial_value + jnp.dot(diff_rows, diff_out, preferred_...  43.3 us
    dot_general x4, matrix products, one_key_block(): jnp.einsum('hmqk,khd->hmqd', exponent.astype(jnp.bfloat16), value_slab, p...  37.2 us
    dot_general x6, matrix products, body(): jnp.dot(segment, weight, preferred_element_type=jnp.float32)  23 us
    reduce_sum x4, other arithmetic, one_key_block(): new_total = block_sum * rescale + jnp.sum(exponent, axis=-1)  19.5 us
    unnamed x39, local copies, waits for them, and re-layouts  12.7 us
    dot_general x4, matrix products, one_key_block(): jnp.einsum('qhmd,khmd->hmqk', query_slab, key_slab, preferred_element_typ...  11 us
  transfers between devices with their start and end apart: 8, of which 6 were waited for; matrix products, arithmetic and copies ran while one was open for 12% of the time, Pallas kernels for 0%

profile of v1, /device:TPU:0, one launch (start us, length us, event | category | flops | bytes accessed | tf_op | source)
XLA Modules:
  0.0 315.2 jit_solution(3632788154810961132)
XLA Ops:
  7.0 14.6 %collective-permute-done = bf16[512,1024]{1,0:T(8,128)(2,1)S(1)} collective-permute-done((bf16[512,1024]{1,0:T(8,128)(2,1)}, bf16[512,1024]{1,0:T(8,128)(2,1)S(1)}, u32[]{:S(2)}, u32[]{:S(2)}) %collective-permute-start) | collective-permute-done | bytes 1048608 | tf_op jit(solution)/shard_map/ppermute | solution.py:171
  22.7 14.3 %collective-permute-done.1 = bf16[512,1024]{1,0:T(8,128)(2,1)} collective-permute-done((bf16[512,1024]{1,0:T(8,128)(2,1)S(1)}, bf16[512,1024]{1,0:T(8,128)(2,1)}, u32[]{:S(2)}, u32[]{:S(2)}) %collective-permute-start.1) | collective-permute-done | bytes 1048608 | tf_op jit(solution)/shard_map/ppermute | solution.py:171
  37.0 14.5 %collective-permute-done.2 = bf16[512,1024]{1,0:T(8,128)(2,1)} collective-permute-done((bf16[512,1024]{1,0:T(8,128)(2,1)}, bf16[512,1024]{1,0:T(8,128)(2,1)}, u32[]{:S(2)}, u32[]{:S(2)}) %collective-permute-start.2) | collective-permute-done | bytes 1048608 | tf_op jit(solution)/shard_map/ppermute | solution.py:171
  59.5 3.2 %copy-done.10 = bf16[512,8192]{1,0:T(8,128)(2,1)} copy-done((bf16[512,8192]{1,0:T(8,128)(2,1)}, bf16[512,8192]{1,0:T(8,128)(2,1)S(1)}, u32[]{:S(2)}) %copy-start.10) | copy-done | bytes 8388632
  66.3 4.3 %fusion.61 = bf16[512,128]{0,1:T(8,128)(2,1)S(1)} fusion(bf16[4096,128]{1,0:T(8,128)(2,1)} %param.21, bf16[512,8192]{1,0:T(8,128)(2,1)} %copy-done.10, s32[]{:T(128)S(6)} %select_n.62), kind=kOutput, calls=%fused_computation.50 | convolution fusion | flops 536936448 | bytes 5373956 | tf_op jit(solution)/shard_map/dot_general | solution.py:176
  70.7 4.0 %fusion.58 = bf16[512,128]{0,1:T(8,128)(2,1)S(1)} fusion(bf16[4096,128]{1,0:T(8,128)(2,1)} %param.20, bf16[512,8192]{1,0:T(8,128)(2,1)} %copy-done.10, s32[]{:T(128)S(6)} %select_n.62), kind=kOutput, calls=%fused_computation.49 | convolution fusion | flops 536936448 | bytes 5373956 | tf_op jit(solution)/shard_map/dot_general | solution.py:176
  77.9 5.5 %collective-permute-start.3 = (bf16[128,256]{0,1:T(8,128)(2,1)}, bf16[128,256]{0,1:T(8,128)(2,1)}, u32[]{:S(2)}, u32[]{:S(2)}) collective-permute-start(bf16[128,256]{0,1:T(8,128)(2,1)} %bitcast.8), channel_id=1, source_target_pairs={{0,4},{4,8},{8,12},{12,16},{16,20},{20,24},{24,28},{1,5},{5,9},{9,... | collective-permute-start | bytes 196616 | tf_op jit(solution)/shard_map/ppermute | solution.py:19
  85.4 5.8 %fusion.46 = bf16[512,384]{0,1:T(8,128)(2,1)} fusion(bf16[4096,384]{1,0:T(8,128)(2,1)} %param.19, bf16[512,8192]{1,0:T(8,128)(2,1)} %copy-done.10, s32[]{:T(128)S(6)} %select_n.62), kind=kOutput, calls=%fused_computation.45 | convolution fusion | flops 1610809344 | bytes 7733252 | tf_op jit(solution)/shard_map/dot_general | solution.py:176
  91.4 4.9 %fusion.49 = bf16[512,256]{1,0:T(8,128)(2,1)} fusion(bf16[4096,256]{1,0:T(8,128)(2,1)} %param.23, bf16[512,8192]{1,0:T(8,128)(2,1)} %copy-done.10, s32[]{:T(128)S(6)} %select_n.62), kind=kOutput, calls=%fused_computation.46 | convolution fusion | flops 1073872896 | bytes 6553604 | tf_op jit(solution)/shard_map/dot_general | solution.py:176
  99.1 2.3 fusion.24
  101.5 2.7 fusion.70
  104.2 5.6 %fusion.88 = f32[512,4096]{1,0:T(8,128)} fusion(bf16[512,384]{0,1:T(8,128)(2,1)S(1)} %bitcast.117, bf16[384,4096]{1,0:T(8,128)(2,1)S(1)} %copy-done), kind=kOutput, calls=%fused_computation.94 | convolution fusion | flops 1610612736 | bytes 11927552 | tf_op jit(solution)/shard_map/dot_general | solution.py:182
  109.8 6.7 %all-gather.3.cloned.1.call-done = bf16[4096,256]{1,0:T(8,128)(2,1)} async-done(((bf16[512,256]{1,0:T(8,128)(2,1)}), bf16[4096,256]{1,0:T(8,128)(2,1)}) %all-gather.3.cloned.1.call-update) | async-done | bytes 2097168 | tf_op jit(solution)/shard_map/all_gather | solution.py:125
  116.5 49.8 %all-gather.5.cloned.1.call-done = bf16[4096,256]{1,0:T(8,128)(2,1)} async-done(((bf16[512,256]{1,0:T(8,128)(2,1)}), bf16[4096,256]{1,0:T(8,128)(2,1)}) %all-gather.5.cloned.1.call-update) | async-done | bytes 2097168 | tf_op jit(solution)/shard_map/all_gather | solution.py:126
  166.3 89.2 %conditional.1 = (f32[4,2,512]{2,1,0:T(2,128)}, f32[4,2,512,64]{2,3,1,0:T(8,128)}) conditional(s32[]{:T(128)} %convert_element_type.55, () %tuple.29, (s32[512]{0:T(512)S(1)}, bf16[512,256]{1,0:T(8,128)(2,1)S(1)}, bf16[4096,256]{1,0:T(8,128)(2,1)}, bf16[4096,256]{1,0:T(8,128)(2,1)}, s32[]{:T(128)}, /*index=5*/s32[]{:T(128)}) %tuple.72), branch_computations={%region_3.4_spmd, %region_4.9_spmd.clone} | conditional | flops 859970048 | bytes 132364824 | solution.py:127
  167.7 4.1 %copy.34 = bf16[4096,256]{0,1:T(8,128)(2,1)} copy(bf16[4096,256]{1,0:T(8,128)(2,1)} %get-tuple-element.232) | data formatting | bytes 4194304 | tf_op jit(solution)/shard_map
  171.8 2.9 copy.33
  176.5 79.0 %while.33 = (s32[]{:T(128)}, f32[4,2,512]{2,1,0:T(2,128)S(1)}, f32[4,2,512]{2,1,0:T(2,128)}, f32[4,2,512,64]{2,3,1,0:T(8,128)}, s32[]{:T(128)}, /*index=5*/s32[]...) while((s32[]{:T(128)}, f32[4,2,512]{2,1,0:T(2,128)S(1)}, ...), condition=%wide.region_8.8_spmd, body=%wide.region_5.7_spmd.sunk | while | flops 859969536 | bytes 122368224 | solution.py:109
  177.1 2.7 fusion.112
  179.9 4.9 %fusion.113 = f32[4,2,128]{2,1,0:T(2,128)S(1)} fusion(f32[4,2,128,4096]{3,2,1,0:T(8,128)S(1)} %get-tuple-element.339, f32[4,2,128]{2,1,0:T(2,128)S(1)} %get-tuple-element.340, pred[4096]{0:T(1024)(128)(4,1)S(1)} %iota_compare_fusion.2), kind=kLoop, calls=%fused_computation.4.clone.1 | loop fusion | flops 20970496 | bytes 16789504 | tf_op jit(solution)/shard_map/cond/branch_1_fun/while/body/while/body/eval_jaxpr/reduce_sum | solution.py:93
  186.9 9.3 %fusion.114 = f32[4,2,512,64]{2,3,1,0:T(8,128)} fusion(f32[4,2,512,64]{2,3,1,0:T(8,128)} %get-tuple-element.359, s32[]{:T(128)S(6)} %select_n.141, bf16[4096,4,64]{0,2,1:T(8,128)(2,1)} %get-tuple-element.377, f32[4,2,128,4096]{3,2,1,0:T(8,128)} %copy-done.2, f32[4,2,128]{2,1,0:T(2,128)S(1)} %get-tuple-element.340, ...), kind=kOutput, calls=%fused_computation.9.clone.1 | convolution fusion | flops 557973504 | bytes 19410948 | tf_op jit(solution)/shard_map/cond/branch_1_fun/while/body/while/body/eval_jaxpr/hmqk,khd->hmqd/dot_general | solution.py:94
  196.9 2.7 fusion.112
  199.7 4.9 %fusion.113 = f32[4,2,128]{2,1,0:T(2,128)S(1)} fusion(f32[4,2,128,4096]{3,2,1,0:T(8,128)S(1)} %get-tuple-element.339, f32[4,2,128]{2,1,0:T(2,128)S(1)} %get-tuple-element.340, pred[4096]{0:T(1024)(128)(4,1)S(1)} %iota_compare_fusion.2), kind=kLoop, calls=%fused_computation.4.clone.1 | loop fusion | flops 20970496 | bytes 16789504 | tf_op jit(solution)/shard_map/cond/branch_1_fun/while/body/while/body/eval_jaxpr/reduce_sum | solution.py:93
  206.7 9.3 %fusion.114 = f32[4,2,512,64]{2,3,1,0:T(8,128)} fusion(f32[4,2,512,64]{2,3,1,0:T(8,128)} %get-tuple-element.359, s32[]{:T(128)S(6)} %select_n.141, bf16[4096,4,64]{0,2,1:T(8,128)(2,1)} %get-tuple-element.377, f32[4,2,128,4096]{3,2,1,0:T(8,128)} %copy-done.2, f32[4,2,128]{2,1,0:T(2,128)S(1)} %get-tuple-element.340, ...), kind=kOutput, calls=%fused_computation.9.clone.1 | convolution fusion | flops 557973504 | bytes 19410948 | tf_op jit(solution)/shard_map/cond/branch_1_fun/while/body/while/body/eval_jaxpr/hmqk,khd->hmqd/dot_general | solution.py:94
  216.7 2.7 fusion.112
  219.4 4.9 %fusion.113 = f32[4,2,128]{2,1,0:T(2,128)S(1)} fusion(f32[4,2,128,4096]{3,2,1,0:T(8,128)S(1)} %get-tuple-element.339, f32[4,2,128]{2,1,0:T(2,128)S(1)} %get-tuple-element.340, pred[4096]{0:T(1024)(128)(4,1)S(1)} %iota_compare_fusion.2), kind=kLoop, calls=%fused_computation.4.clone.1 | loop fusion | flops 20970496 | bytes 16789504 | tf_op jit(solution)/shard_map/cond/branch_1_fun/while/body/while/body/eval_jaxpr/reduce_sum | solution.py:93
  226.4 9.3 %fusion.114 = f32[4,2,512,64]{2,3,1,0:T(8,128)} fusion(f32[4,2,512,64]{2,3,1,0:T(8,128)} %get-tuple-element.359, s32[]{:T(128)S(6)} %select_n.141, bf16[4096,4,64]{0,2,1:T(8,128)(2,1)} %get-tuple-element.377, f32[4,2,128,4096]{3,2,1,0:T(8,128)} %copy-done.2, f32[4,2,128]{2,1,0:T(2,128)S(1)} %get-tuple-element.340, ...), kind=kOutput, calls=%fused_computation.9.clone.1 | convolution fusion | flops 557973504 | bytes 19410948 | tf_op jit(solution)/shard_map/cond/branch_1_fun/while/body/while/body/eval_jaxpr/hmqk,khd->hmqd/dot_general | solution.py:94
  236.4 2.7 fusion.112
  239.2 4.9 %fusion.113 = f32[4,2,128]{2,1,0:T(2,128)S(1)} fusion(f32[4,2,128,4096]{3,2,1,0:T(8,128)S(1)} %get-tuple-element.339, f32[4,2,128]{2,1,0:T(2,128)S(1)} %get-tuple-element.340, pred[4096]{0:T(1024)(128)(4,1)S(1)} %iota_compare_fusion.2), kind=kLoop, calls=%fused_computation.4.clone.1 | loop fusion | flops 20970496 | bytes 16789504 | tf_op jit(solution)/shard_map/cond/branch_1_fun/while/body/while/body/eval_jaxpr/reduce_sum | solution.py:93
  246.2 9.3 %fusion.114 = f32[4,2,512,64]{2,3,1,0:T(8,128)} fusion(f32[4,2,512,64]{2,3,1,0:T(8,128)} %get-tuple-element.359, s32[]{:T(128)S(6)} %select_n.141, bf16[4096,4,64]{0,2,1:T(8,128)(2,1)} %get-tuple-element.377, f32[4,2,128,4096]{3,2,1,0:T(8,128)} %copy-done.2, f32[4,2,128]{2,1,0:T(2,128)S(1)} %get-tuple-element.340, ...), kind=kOutput, calls=%fused_computation.9.clone.1 | convolution fusion | flops 557973504 | bytes 19410948 | tf_op jit(solution)/shard_map/cond/branch_1_fun/while/body/while/body/eval_jaxpr/hmqk,khd->hmqd/dot_general | solution.py:94
  258.0 7.4 %add_convert_fusion = bf16[512,4096]{1,0:T(8,128)(2,1)} fusion(f32[512,4096]{1,0:T(8,128)} %fusion.88, bf16[512,256]{0,1:T(8,128)(2,1)S(1)} %bitcast.112, bf16[256,4096]{1,0:T(8,128)(2,1)} %param.29), kind=kOutput, calls=%fused_computation.23 | convolution fusion | flops 1077936128 | bytes 14942208 | tf_op jit(solution)/shard_map/dot_general | solution.py:184
  265.4 43.3 %reduce-scatter.2.cloned.1.call-done = bf16[128,4096]{1,0:T(8,128)(2,1)} async-done(((bf16[512,4096]{1,0:T(8,128)(2,1)}), bf16[128,4096]{1,0:T(8,128)(2,1)}) %reduce-scatter.2.cloned.1.call-update) | async-done | bytes 1048592 | tf_op jit(solution)/shard_map/reduce_scatter | solution.py:183
  (104 shorter events, 36.8 us)
Async XLA Ops:
  6.5 97.6 %copy-start = (bf16[384,4096]{1,0:T(8,128)(2,1)S(1)}, bf16[384,4096]{1,0:T(8,128)(2,1)}, u32[]{:S(2)}) copy-start(bf16[384,4096]{1,0:T(8,128)(2,1)} %param.28) | copy-start | bytes 9437188
  6.5 109.9 %all-gather.3.cloned.1.call-start = ((), (), s32[]{:S(2)}) async-start(), calls=%async_computation.1 | async-start | bytes 2359296 | tf_op jit(solution)/shard_map/all_gather | solution.py:125
  6.5 15.1 %collective-permute-start = (bf16[512,1024]{1,0:T(8,128)(2,1)}, bf16[512,1024]{1,0:T(8,128)(2,1)S(1)}, u32[]{:S(2)}, u32[]{:S(2)}) collective-permute-start(bf16[512,1024]{1,0:T(8,128)(2,1)} %param.17), channel_id=1, source_target_pairs={{0,1},{1,2},{2,3},{3,0},{4,5},{5,6},{6,7},{7,4},{8,9},{9,10},{10,1... | collective-permute-start | bytes 3145736 | tf_op jit(solution)/shard_map/ppermute | solution.py:171
  21.6 1.0 copy-start.4
  22.6 14.3 %collective-permute-start.1 = (bf16[512,1024]{1,0:T(8,128)(2,1)S(1)}, bf16[512,1024]{1,0:T(8,128)(2,1)}, u32[]{:S(2)}, u32[]{:S(2)}) collective-permute-start(bf16[512,1024]{1,0:T(8,128)(2,1)S(1)} %collective-permute-done), channel_id=1, source_target_pairs={{0,1},{1,2},{2,3},{3,0},{4,5},{5,6},{6,7},{7,4},{8,9},{9,10},{10,1... | collective-permute-start | bytes 3145736 | tf_op jit(solution)/shard_map/ppermute | solution.py:171
  36.9 14.5 %collective-permute-start.2 = (bf16[512,1024]{1,0:T(8,128)(2,1)}, bf16[512,1024]{1,0:T(8,128)(2,1)}, u32[]{:S(2)}, u32[]{:S(2)}) collective-permute-start(bf16[512,1024]{1,0:T(8,128)(2,1)} %collective-permute-done.1), channel_id=1, source_target_pairs={{0,1},{1,2},{2,3},{3,0},{4,5},{5,6},{6,7},{7,4},{8,9},{9,10},{10,1... | collective-permute-start | bytes 3145736 | tf_op jit(solution)/shard_map/ppermute | solution.py:171
  36.9 22.3 %copy-start.5 = (bf16[512,1024]{1,0:T(8,128)(2,1)S(1)}, bf16[512,1024]{1,0:T(8,128)(2,1)}, u32[]{:S(2)}) copy-start(bf16[512,1024]{1,0:T(8,128)(2,1)} %copy-done.4) | copy-start | bytes 3145732
  36.9 22.4 %copy-start.3 = (bf16[512,1024]{1,0:T(8,128)(2,1)S(1)}, bf16[512,1024]{1,0:T(8,128)(2,1)}, u32[]{:S(2)}) copy-start(bf16[512,1024]{1,0:T(8,128)(2,1)} %param.17) | copy-start | bytes 3145732
  36.9 25.7 %copy-start.14 = (bf16[4096,256]{1,0:T(8,128)(2,1)S(1)}, bf16[4096,256]{1,0:T(8,128)(2,1)}, u32[]{:S(2)}) copy-start(bf16[4096,256]{1,0:T(8,128)(2,1)} %param.24) | copy-start | bytes 6291460
  56.7 8.7 %copy-start.16 = (f32[6]{0:T(128)S(1)}, f32[6]{0:T(128)}, u32[]{:S(2)}) copy-start(f32[6]{0:T(128)} %param.22) | copy-start | bytes 76
  59.5 3.2 %copy-start.10 = (bf16[512,8192]{1,0:T(8,128)(2,1)}, bf16[512,8192]{1,0:T(8,128)(2,1)S(1)}, u32[]{:S(2)}) copy-start(bf16[512,8192]{1,0:T(8,128)(2,1)S(1)} %constant_dynamic-update-slice_fusion.1) | copy-start | bytes 25165828
  64.7 101.6 %all-gather.5.cloned.1.call-start = ((), (), s32[]{:S(2)}) async-start(), calls=%async_computation.2 | async-start | bytes 2359296 | tf_op jit(solution)/shard_map/all_gather | solution.py:126
  65.5 17.9 %copy-start.11 = (bf16[512,8192]{1,0:T(8,128)(2,1)S(1)}, bf16[512,8192]{1,0:T(8,128)(2,1)}, u32[]{:S(2)}) copy-start(bf16[512,8192]{1,0:T(8,128)(2,1)} %copy-done.10) | copy-start | bytes 25165828
  65.5 17.9 %copy-start.15 = (bf16[4096,256]{1,0:T(8,128)(2,1)S(1)}, bf16[4096,256]{1,0:T(8,128)(2,1)}, u32[]{:S(2)}) copy-start(bf16[4096,256]{1,0:T(8,128)(2,1)} %param.25) | copy-start | bytes 6291460
  70.7 4.1 %copy-start.6 = (bf16[512,128]{0,1:T(8,128)(2,1)}, bf16[512,128]{0,1:T(8,128)(2,1)S(1)}, u32[]{:S(2)}) copy-start(bf16[512,128]{0,1:T(8,128)(2,1)S(1)} %fusion.61) | copy-start | bytes 393220
  74.7 0.7 copy-start.7
  76.6 19.7 %collective-permute-start.4 = (bf16[128,256]{0,1:T(8,128)(2,1)}, bf16[128,256]{0,1:T(8,128)(2,1)}, u32[]{:S(2)}, u32[]{:S(2)}) collective-permute-start(bf16[128,256]{0,1:T(8,128)(2,1)} %bitcast.10), channel_id=1, source_target_pairs={{4,0},{8,4},{12,8},{16,12},{20,16},{24,20},{28,24},{5,1},{9,5},{13... | collective-permute-start | bytes 196616 | tf_op jit(solution)/shard_map/ppermute | solution.py:22
  77.9 18.4 %collective-permute-start.3 = (bf16[128,256]{0,1:T(8,128)(2,1)}, bf16[128,256]{0,1:T(8,128)(2,1)}, u32[]{:S(2)}, u32[]{:S(2)}) collective-permute-start(bf16[128,256]{0,1:T(8,128)(2,1)} %bitcast.8), channel_id=1, source_target_pairs={{0,4},{4,8},{8,12},{12,16},{16,20},{20,24},{24,28},{1,5},{5,9},{9,... | collective-permute-start | bytes 196616 | tf_op jit(solution)/shard_map/ppermute | solution.py:19
  91.2 217.5 %reduce-scatter.2.cloned.1.call-start = ((), (), s32[]{:S(2)}) async-start(), calls=%async_computation.3 | async-start | bytes 5242880 | tf_op jit(solution)/shard_map/reduce_scatter | solution.py:183
  91.4 5.9 %copy-start.8 = (bf16[512,384]{0,1:T(8,128)(2,1)S(1)}, bf16[512,384]{0,1:T(8,128)(2,1)}, u32[]{:S(2)}) copy-start(bf16[512,384]{0,1:T(8,128)(2,1)} %fusion.46) | copy-start | bytes 1179652
  104.2 62.1 %copy-start.9 = (bf16[512,256]{1,0:T(8,128)(2,1)S(1)}, bf16[512,256]{1,0:T(8,128)(2,1)}, u32[]{:S(2)}) copy-start(bf16[512,256]{1,0:T(8,128)(2,1)} %fusion.49) | copy-start | bytes 786436
  166.3 91.4 %copy-start.12 = (f32[4]{0:T(128)S(1)}, f32[4]{0:T(128)}, u32[]{:S(2)}) copy-start(f32[4]{0:T(128)} %param.26) | copy-start | bytes 52
  166.3 91.6 %copy-start.13 = (f32[64]{0:T(128)S(1)}, f32[64]{0:T(128)}, u32[]{:S(2)}) copy-start(f32[64]{0:T(128)} %param.27) | copy-start | bytes 772
  179.9 5.7 %copy-start.2 = (f32[4,2,128,4096]{3,2,1,0:T(8,128)}, f32[4,2,128,4096]{3,2,1,0:T(8,128)S(1)}, u32[]{:S(2)}) copy-start(f32[4,2,128,4096]{3,2,1,0:T(8,128)S(1)} %get-tuple-element.339) | copy-start | bytes 50331652 | tf_op jit(solution)/shard_map/cond/branch_1_fun/while
  199.6 5.7 %copy-start.2 = (f32[4,2,128,4096]{3,2,1,0:T(8,128)}, f32[4,2,128,4096]{3,2,1,0:T(8,128)S(1)}, u32[]{:S(2)}) copy-start(f32[4,2,128,4096]{3,2,1,0:T(8,128)S(1)} %get-tuple-element.339) | copy-start | bytes 50331652 | tf_op jit(solution)/shard_map/cond/branch_1_fun/while
  219.4 5.7 %copy-start.2 = (f32[4,2,128,4096]{3,2,1,0:T(8,128)}, f32[4,2,128,4096]{3,2,1,0:T(8,128)S(1)}, u32[]{:S(2)}) copy-start(f32[4,2,128,4096]{3,2,1,0:T(8,128)S(1)} %get-tuple-element.339) | copy-start | bytes 50331652 | tf_op jit(solution)/shard_map/cond/branch_1_fun/while
  239.2 5.7 %copy-start.2 = (f32[4,2,128,4096]{3,2,1,0:T(8,128)}, f32[4,2,128,4096]{3,2,1,0:T(8,128)S(1)}, u32[]{:S(2)}) copy-start(f32[4,2,128,4096]{3,2,1,0:T(8,128)S(1)} %get-tuple-element.339) | copy-start | bytes 50331652 | tf_op jit(solution)/shard_map/cond/branch_1_fun/while
  258.0 50.7 %copy-start.1 = (bf16[384,4096]{1,0:T(8,128)(2,1)S(1)}, bf16[384,4096]{1,0:T(8,128)(2,1)}, u32[]{:S(2)}) copy-start(bf16[384,4096]{1,0:T(8,128)(2,1)} %param.28) | copy-start | bytes 9437188
Sparse Core Ops, SparseCore 0:
  64.8 51.6 all-gather.2
  118.6 47.6 all-gather.4
  265.6 43.1 reduce-scatter.1
